TPU v7x, 32 devices: a whole 2x2x4 slice. The times are simulated.
32 devices in a mesh: grp: 2 (over y), sp: 4 (over z), fs: 2 (over x), tp: 2 (over core).
Axes of the slice: x: 2, y: 2, z: 4, core: 2. Of those that a mesh axis runs over, the one named last changes fastest.
Arguments:
- tokens: bfloat16 [4, 2048, 2048], P(('grp', 'fs'), ('sp', 'tp')), parts along dimension 0, may hold values from -6 to 6
- norm_gain: float32 [2048], replicated, may hold values from 0.1 to 1.9
- w_bgate: bfloat16 [2048, 2048], P(('sp', 'fs'), 'tp'), may hold values from -0.125 to 0.125
- w_cgate: bfloat16 [2048, 2048], P(('sp', 'fs'), 'tp'), may hold values from -0.125 to 0.125
- w_conv_in: bfloat16 [2048, 2048], P(('sp', 'fs'), 'tp'), may hold values from -0.125 to 0.125
- conv_taps: bfloat16 [3, 2048], P(None, 'tp'), may hold values from -3.5 to 3.5
- w_query: bfloat16 [2048, 2048], P(('sp', 'fs'), 'tp'), may hold values from -0.13258252 to 0.13258252
- w_key: bfloat16 [2048, 256], P(('sp', 'fs'), 'tp'), may hold values from -4.02167 to 4.02167
- w_value: bfloat16 [2048, 256], P(('sp', 'fs'), 'tp'), may hold values from -0.125 to 0.125
- sink_logits: float32 [32], P('tp'), may hold values from 1 to 6
- conv_out_weight: bfloat16 [2048, 2048], P('tp', ('sp', 'fs')), may hold values from -0.125 to 0.125
- attn_out_weight: bfloat16 [2048, 2048], P('tp', ('sp', 'fs')), may hold values from -0.75 to 0.75
Outputs:
- mixed: bfloat16 [4, 2048, 2048], P(('grp', 'fs'), ('sp', 'tp')), parts along dimension 0
There are 2 independent parts, one for each index of `grp`. A program takes and returns all parts, laid end to end along the dimension named above; an argument that names none is the same for every part. Nothing has to cross between parts.
All inputs are finite; a program needn't handle non-finite values.
Results may differ from a plain program's by a relative error of at most 0.014.
The roundings to bfloat16 on the way count: a program that leaves them out, or rounds other values in their place, can miss the bound.
Values may be sent and summed in bfloat16 or wider, within the bound.
A program may use at most 128 MiB of HBM per device.

v0:
```python
import functools

import jax
import jax.numpy as jnp
from jax import lax
from jax.experimental import pallas as pl
from jax.experimental.pallas import tpu as pltpu
from jax.sharding import PartitionSpec as P

HEAD = 64
WINDOW = 128
TAPS = 3
LANES = 128
HALO = 16
TILE = 256
UNIT = 16
MESH = pl.DeviceIdType.MESH

epsilon = 1e-06


def part(count, sixteenths):
    return max(UNIT, count * sixteenths // 16 // UNIT * UNIT)


def kernel(
    n,
    m,
    normed,
    w_key,
    w_value,
    w_query,
    w_cgate,
    w_conv_in,
    w_bgate,
    conv_weight,
    attn_weight,
    taps,
    sink,
    out,
    w_in,
    w_out,
    rows,
    query,
    keys,
    gate,
    mine_conv,
    conv,
    attended,
    total,
    partial,
    theirs,
    local_sem,
    rows_send,
    rows_recv,
    halo_send,
    halo_recv,
    trade_send,
    trade_recv,
    in_send,
    in_recv,
    in_on,
    in_y_send,
    in_y_recv,
    z_send,
    z_on,
    x_send,
    out_recv,
    y_send,
    y_recv,
    give_send,
    give_recv,
    swap_send,
    swap_recv,
):
    inputs = (w_key, w_value, w_query, w_cgate, w_conv_in, w_bgate)
    outputs = (conv_weight, attn_weight)
    own, features = normed.shape
    length = 2 * own
    span = WINDOW + length
    depth, kv = w_key.shape
    width = w_query.shape[1]
    slim = width // m
    across_out = conv_weight.shape[1]
    heads = slim // HEAD
    per_kv = width // kv
    chunks = n * m
    firsts = [0, kv] + [2 * kv + i * slim for i in range(4)]
    sizes = [kv, kv] + [slim] * 4
    in_alone = [part(depth, 7)] * 6
    out_alone = [part(width, 7), part(width, 5)]

    grp, sp = lax.axis_index("grp"), lax.axis_index("sp")
    fs, tp = lax.axis_index("fs"), lax.axis_index("tp")
    mine = sp * m + fs

    def loop(low, high, body):
        def step(i, carry):
            body(i)
            return carry

        lax.fori_loop(low, high, step, 0)

    def remote(source, target, send, recv, where):
        return pltpu.make_async_remote_copy(
            source, target, send, recv, device_id=where, device_id_type=MESH
        )

    def to_sp(d):
        return {"sp": lax.rem(sp + d, n)}

    def to_fs(e):
        return {"fs": lax.rem(fs + e, m)}

    other_core = {"tp": 1 - tp}
    other_grp = {"grp": 1 - grp}

    def columns(j, f):
        if j < 2:
            return pl.ds(0, kv)
        return pl.ds(pl.multiple_of(f * slim, LANES), slim)

    def kept(j):
        return pl.ds(firsts[j], sizes[j])

    fills = [
        pltpu.make_async_copy(
            inputs[j].at[:, columns(j, fs)], w_in.at[mine, :, kept(j)], local_sem.at[j]
        )
        for j in range(6)
    ] + [
        pltpu.make_async_copy(outputs[j], w_out.at[j, mine], local_sem.at[6 + j]) for j in range(2)
    ]
    at_own = pl.multiple_of(WINDOW + tp * own, LANES)
    at_other = pl.multiple_of(WINDOW + (1 - tp) * own, LANES)
    fills.append(
        pltpu.make_async_copy(normed, rows.at[fs, pl.ds(at_own, own)], local_sem.at[8])
    )
    for fill in fills:
        fill.start()

    @pl.when(sp == 0)
    def _():
        for i in range(m):
            rows[i, pl.ds(0, WINDOW), :] = jnp.zeros((WINDOW, features), jnp.bfloat16)

    barrier = pltpu.get_barrier_semaphore()

    def greet(where):
        pl.semaphore_signal(barrier, inc=1, device_id=where, device_id_type=MESH)

    loop(1, n, lambda d: greet(to_sp(d)))
    loop(1, m, lambda e: greet(to_fs(e)))
    greet(other_grp)
    greet(other_core)
    pl.semaphore_wait(barrier, n + m)

    def trade(j, e):
        f = lax.rem(fs + e, m)
        return remote(
            inputs[j].at[:, columns(j, f)],
            w_in.at[mine, :, kept(j)],
            trade_send.at[j, e],
            trade_recv.at[j, fs],
            {"fs": f},
        )

    def trade_arrival(j, f):
        piece = w_in.at[sp * m + f, :, kept(j)]
        return remote(piece, piece, trade_send.at[j, 0], trade_recv.at[j, f], to_fs(1))

    def in_rows(j):
        return pl.ds(pl.multiple_of(grp * in_alone[j], UNIT), depth - in_alone[j])

    def in_lone(j, group):
        return pl.ds(
            pl.multiple_of(group * (depth - in_alone[j]), UNIT), in_alone[j]
        )

    steps = (1, -1, 2, -2)

    def near(body):
        for slot, by in enumerate(steps):
            there = sp + by

            @pl.when((there >= 0) & (there < n))
            def _():
                body(slot, jnp.clip(there, 0, n - 1))

    def hand_on(s, body):
        @pl.when((sp - s >= 2) & (sp < n - 1))
        def _():
            body(jnp.minimum(sp + 1, n - 1))

        @pl.when((s - sp >= 2) & (sp > 0))
        def _():
            body(jnp.maximum(sp - 1, 0))

    def other_sp(d):
        return lax.rem(jnp.where(2 * sp >= n, sp - d + n, sp + d), n)

    def in_z(j, slot, chunk, f, there):
        piece = w_in.at[chunk, in_rows(j), kept(j)]
        return remote(
            piece, piece, in_send.at[j, slot, f], in_recv.at[j, chunk], {"sp": there}
        )

    def in_hand(j, chunk, there):
        piece = w_in.at[chunk, in_rows(j), kept(j)]
        return remote(piece, piece, in_on.at[j, chunk], in_recv.at[j, chunk], {"sp": there})

    def in_y(j, chunk, group):
        piece = w_in.at[chunk, in_lone(j, group), kept(j)]
        return remote(piece, piece, in_y_send.at[j, chunk], in_y_recv.at[j, chunk], other_grp)

    def rows_copy(source, f, core, send, where):
        at = pl.multiple_of(WINDOW + core * own, LANES)
        return remote(
            source, rows.at[f, pl.ds(at, own)], rows_send.at[send], rows_recv.at[f, core], where
        )

    def rows_x(e):
        return rows_copy(normed, fs, tp, e, to_fs(e))

    def rows_core(f):
        return rows_copy(rows.at[f, pl.ds(at_own, own)], f, tp, m + f, other_core)

    def halo_copy(source, f, send, where):
        return remote(
            source, rows.at[f, pl.ds(0, WINDOW)], halo_send.at[send], halo_recv.at[f], where
        )

    def halo_here(f):
        return rows.at[f, pl.ds(0, WINDOW)]

    onward = halo_copy(normed.at[pl.ds(own - WINDOW, WINDOW)], fs, 0, to_sp(1))

    def out_rows(j):
        return pl.ds(pl.multiple_of(grp * out_alone[j], UNIT), width - out_alone[j])

    def out_lone(j, group):
        return pl.ds(pl.multiple_of(group * (width - out_alone[j]), UNIT), out_alone[j])

    def along_z(j, slot, there):
        piece = w_out.at[j, mine, out_rows(j)]
        return remote(piece, piece, z_send.at[j, slot], out_recv.at[j, mine], {"sp": there})

    def out_hand(j, chunk, there):
        piece = w_out.at[j, chunk, out_rows(j)]
        return remote(piece, piece, z_on.at[j, chunk], out_recv.at[j, chunk], {"sp": there})

    def along_x(j, s, e, chunk):
        piece = w_out.at[j, chunk, out_rows(j)]
        return remote(piece, piece, x_send.at[j, s, e], out_recv.at[j, chunk], to_fs(e))

    def arrival(j, chunk):
        piece = w_out.at[j, chunk, out_rows(j)]
        return remote(piece, piece, z_send.at[j, 0], out_recv.at[j, chunk], to_sp(1))

    def along_y(j, chunk, group):
        piece = w_out.at[j, chunk, out_lone(j, group)]
        return remote(piece, piece, y_send.at[j, chunk], y_recv.at[j, chunk], other_grp)

    def own_in(j):
        fills[j].wait()
        near(lambda slot, there: in_z(j, slot, mine, fs, there).start())

    def traded_in(j):
        def traded(e):
            f = lax.rem(fs + e, m)
            trade_arrival(j, f).wait_recv()
            near(lambda slot, there: in_z(j, slot, sp * m + f, f, there).start())

        loop(1, m, traded)

    def own_out(j):
        fills[6 + j].wait()
        near(lambda slot, there: along_z(j, slot, there).start())
        loop(1, m, lambda e: along_x(j, sp, e, mine).start())

    for j in range(3):
        loop(1, m, lambda e: trade(j, e).start())
        own_in(j)

    @pl.when((tp == 1) & (sp < n - 1))
    def _():
        onward.start()

    loop(1, m, lambda e: rows_x(e).start())
    for j in range(3, 6):
        loop(1, m, lambda e: trade(j, e).start())
    fills[8].wait()
    rows_core(fs).start()
    for j in range(3):
        traded_in(j)
    own_in(3)
    own_out(0)
    own_in(4)
    traded_in(3)
    own_in(5)
    traded_in(4)
    traded_in(5)
    own_out(1)

    def rows_on(e):
        f = lax.rem(fs + e, m)
        rows_copy(rows.at[f, pl.ds(at_own, own)], f, tp, 0, to_fs(e)).wait_recv()
        rows_core(f).start()

    loop(1, m, rows_on)

    @pl.when((tp == 1) & (sp > 0))
    def _():
        halo_copy(halo_here(fs), fs, 0, other_core).wait_recv()
        halo_copy(halo_here(fs), fs, 1 + fs, other_core).start()
        loop(1, m, lambda e: halo_copy(halo_here(fs), fs, m + e, to_fs(e)).start())

        def pass_on(e):
            f = lax.rem(fs + e, m)
            halo_copy(halo_here(f), f, 0, other_core).wait_recv()
            halo_copy(halo_here(f), f, 1 + f, other_core).start()

        loop(1, m, pass_on)

    def rows_in(f):
        piece = rows.at[f, pl.ds(at_other, own)]
        remote(piece, piece, rows_send.at[0], rows_recv.at[f, 1 - tp], other_core).wait_recv()

    loop(0, m, rows_in)

    @pl.when((tp == 0) & (sp > 0))
    def _():
        loop(0, m, lambda f: halo_copy(halo_here(f), f, 0, other_core).wait_recv())

    def in_from_z(j):
        def body(i):
            s = other_sp(1 + i // m)
            chunk = s * m + lax.rem(fs + i, m)
            in_hand(j, chunk, sp).wait_recv()
            hand_on(s, lambda there: in_hand(j, chunk, there).start())
            in_y(j, chunk, grp).start()

        loop(0, (n - 1) * m, body)

    def in_from_y(j):
        def body(i):
            s = other_sp(1 + i // m)
            in_y(j, s * m + lax.rem(fs + i, m), 1 - grp).wait_recv()

        loop(0, (n - 1) * m, body)

    def from_z(j):
        def body(d):
            s = other_sp(d)
            chunk = s * m + fs
            arrival(j, chunk).wait_recv()
            hand_on(s, lambda there: out_hand(j, chunk, there).start())
            loop(1, m, lambda e: along_x(j, s, e, chunk).start())
            along_y(j, chunk, grp).start()

        loop(1, n, body)

    def from_x(j):
        def body(d):
            s = lax.rem(sp + d, n)

            def inner(e):
                chunk = s * m + lax.rem(fs + e, m)
                arrival(j, chunk).wait_recv()
                along_y(j, chunk, grp).start()

            loop(1, m, inner)

        loop(0, n, body)

    def from_y(j):
        loop(
            1,
            chunks,
            lambda d: along_y(j, lax.rem(mine + d, chunks), 1 - grp).wait_recv(),
        )

    def project(i, first, count):
        block = w_in[:, :, pl.ds(first, count)].reshape(chunks * depth, count)
        return jnp.dot(rows[i], block, preferred_element_type=jnp.float32).astype(jnp.bfloat16)

    def tiles(body):
        step = min(TILE, slim)
        for i in range(m):
            loop(0, slim // step, lambda t: body(i, pl.multiple_of(t * step, LANES), step))

    kv_head = fs * heads // per_kv

    def do_keys():
        for i in range(m):
            both = project(i, 0, 2 * kv).astype(jnp.float32)
            picked = []
            for base in (0, kv):
                one = both[:, base : base + HEAD]
                for h in range(1, kv // HEAD):
                    at = base + h * HEAD
                    one = jnp.where(kv_head == h, both[:, at : at + HEAD], one)
                picked.append(one)
            keys[i] = jnp.concatenate(picked, axis=1).astype(jnp.bfloat16)

    def do_query():
        def body(i, at, step):
            query[i, :, pl.ds(at, step)] = project(i, firsts[2] + at, step)

        tiles(body)

    def result(which, f):
        return mine_conv.at[f] if which == 0 else query.at[f, pl.ds(WINDOW, length)]

    def give(which, e):
        full = (conv, attended)[which]
        f = lax.rem(fs + e, m)
        here = pl.ds(pl.multiple_of(fs * slim, LANES), slim)
        return remote(
            result(which, f), full.at[:, here], give_send.at[which, e], give_recv.at[which, fs], {"fs": f}
        )

    def given(which, e):
        full = (conv, attended)[which]
        f = lax.rem(fs + e, m)
        piece = full.at[:, pl.ds(pl.multiple_of(f * slim, LANES), slim)]
        return remote(piece, piece, give_send.at[which, 0], give_recv.at[which, f], to_fs(e))

    def keep(which):
        full = (conv, attended)[which]
        full[:, pl.ds(pl.multiple_of(fs * slim, LANES), slim)] = result(which, fs)[...]

    def do_attention():
        pairs = 2 * HEAD
        blocks = length // WINDOW
        count = heads // 2
        place_q = lax.broadcasted_iota(jnp.int32, (WINDOW, 2 * WINDOW), 0)
        place_k = lax.broadcasted_iota(jnp.int32, (WINDOW, 2 * WINDOW), 1)
        banded = (place_k > place_q) & (place_k <= place_q + WINDOW)
        for i in range(m):

            def body(b):
                row = pl.multiple_of(b * WINDOW, WINDOW)
                band = keys[i, pl.ds(row, 2 * WINDOW), :]
                key, value = band[:, :HEAD], band[:, HEAD:]
                least = jnp.where((sp == 0) & (b == 0), WINDOW, 0)
                allowed = banded & (place_k >= least)
                for p in range(count):
                    at = p * pairs
                    both = query[i, pl.ds(row + WINDOW, WINDOW), pl.ds(at, pairs)]
                    results = []
                    for half in range(2):
                        one = both[:, half * HEAD : (half + 1) * HEAD]
                        scores = lax.dot_general(
                            one, key, (((1,), (1,)), ((), ())), preferred_element_type=jnp.float32
                        ) * (1.0 / HEAD**0.5)
                        scores = jnp.where(allowed, scores, -jnp.inf)
                        logit = sink[fs * heads + 2 * p + half]
                        peak = jnp.maximum(jnp.max(scores, axis=-1, keepdims=True), logit)
                        powers = jnp.exp(scores - peak)
                        norm = jnp.sum(powers, axis=-1, keepdims=True) + jnp.exp(logit - peak)
                        probs = (powers / norm).astype(jnp.bfloat16)
                        results.append(jnp.dot(probs, value, preferred_element_type=jnp.float32))
                    query[i, pl.ds(row + WINDOW, WINDOW), pl.ds(at, pairs)] = jnp.concatenate(
                        results, axis=1
                    ).astype(jnp.bfloat16)

            loop(0, blocks, body)

    def do_gate():
        def body(i, at, step):
            gate[i, :, pl.ds(at, step)] = project(i, firsts[3] + at, step)

        tiles(body)

    def do_gated():
        def body(i, at, step):
            values = project(i, firsts[4] + at, step)
            product = gate[i, :, pl.ds(at, step)].astype(jnp.float32) * values.astype(jnp.float32)
            gate[i, :, pl.ds(at, step)] = product.astype(jnp.bfloat16)

        tiles(body)

    def do_conv():
        def body(i, at, step):
            outer = project(i, firsts[5] + at, step)[WINDOW:].astype(jnp.float32)
            mixed = None
            gated = gate[i, pl.ds(WINDOW - HALO, HALO + length), pl.ds(at, step)].astype(jnp.float32)
            for which in range(TAPS):
                there = pl.multiple_of(fs * slim + at, LANES)
                tap = taps[pl.ds(which, 1), pl.ds(there, step)].astype(jnp.float32)
                low = HALO - TAPS + 1 + which
                term = tap * gated[low : low + length]
                mixed = term if mixed is None else mixed + term
            mine_conv[i, :, pl.ds(at, step)] = (outer * mixed).astype(jnp.bfloat16)

        tiles(body)

    per = max(1, LANES // across_out)
    step_out = per * across_out
    turns = chunks // per

    def term(which, left, low, count, t):
        block = jnp.concatenate([w_out[which, t * per + i] for i in range(per)], axis=1)
        return jnp.dot(left[pl.ds(low, count), :], block, preferred_element_type=jnp.float32)

    def piece_of(t):
        return pl.ds(pl.multiple_of(t * step_out, LANES), step_out)

    def do_first():
        def body(t):
            total[:, piece_of(t)] = term(0, conv, 0, length, t)

        loop(0, turns, body)

    def swap(t):
        return remote(
            partial.at[:, piece_of(t)],
            theirs.at[:, piece_of(t)],
            swap_send.at[t],
            swap_recv.at[t],
            other_core,
        )

    def work(j):
        if j == 1:
            do_keys()
        if j == 2:
            do_query()
            do_attention()
        if j == 3:
            loop(1, m, lambda e: give(1, e).start())
            keep(1)
            do_gate()
        if j == 4:
            do_gated()
        if j == 5:
            do_conv()

    order = (0, 1, 2, 3, 6, 4, 5, 7)
    for step in range(10):
        if step < 8:
            item = order[step]
            in_from_z(item) if item < 6 else from_z(item - 6)
        if 1 <= step < 9 and order[step - 1] >= 6:
            from_x(order[step - 1] - 6)
        if step >= 2:
            item = order[step - 2]
            if item < 6:
                in_from_y(item)
                work(item)
            elif item == 6:
                from_y(0)
            else:
                loop(1, m, lambda e: given(0, e).wait_recv())
                do_first()
                loop(1, m, lambda e: given(1, e).wait_recv())
                from_y(1)
        if step == 8:
            loop(1, m, lambda e: give(0, e).start())
            keep(0)

    low_mine = pl.multiple_of(tp * own, LANES)
    low_other = pl.multiple_of((1 - tp) * own, LANES)

    def final(t):
        partial[:, piece_of(t)] = (
            total[pl.ds(low_other, own), piece_of(t)] + term(1, attended, low_other, own, t)
        ).astype(jnp.bfloat16)
        total[pl.ds(low_mine, own), piece_of(t)] = (
            (total[pl.ds(low_mine, own), piece_of(t)] + term(1, attended, low_mine, own, t))
            .astype(jnp.bfloat16)
            .astype(jnp.float32)
        )
        swap(t).start()

    loop(0, turns, final)

    def add(t):
        swap(t).wait()
        out[:, piece_of(t)] = (
            total[pl.ds(low_mine, own), piece_of(t)] + theirs[:, piece_of(t)].astype(jnp.float32)
        ).astype(jnp.bfloat16)

    loop(0, turns, add)

    for j in range(6):
        loop(1, m, lambda e: trade(j, e).wait_send())
        for f in range(m):
            near(lambda slot, there: in_z(j, slot, sp * m + f, f, there).wait_send())

        def in_y_done(i):
            s = other_sp(1 + i // m)
            chunk = s * m + lax.rem(fs + i, m)
            in_y(j, chunk, grp).wait_send()
            hand_on(s, lambda there: in_hand(j, chunk, there).wait_send())

        loop(0, (n - 1) * m, in_y_done)
    for j in range(2):
        near(lambda slot, there: along_z(j, slot, there).wait_send())

        def x_done(d):
            s = lax.rem(sp + d, n)
            hand_on(s, lambda there: out_hand(j, s * m + fs, there).wait_send())
            loop(1, m, lambda e: along_x(j, s, e, s * m + fs).wait_send())

        loop(0, n, x_done)
        loop(1, chunks, lambda d: along_y(j, lax.rem(mine + d, chunks), grp).wait_send())
        loop(1, m, lambda e: give(j, e).wait_send())
    loop(1, m, lambda e: rows_x(e).wait_send())
    loop(0, m, lambda f: rows_core(f).wait_send())

    @pl.when((tp == 1) & (sp < n - 1))
    def _():
        onward.wait_send()

    @pl.when((tp == 1) & (sp > 0))
    def _():
        loop(1, m, lambda e: halo_copy(halo_here(fs), fs, m + e, to_fs(e)).wait_send())
        loop(0, m, lambda f: halo_copy(halo_here(f), f, 1 + f, other_core).wait_send())


def local(
    n,
    m,
    tokens,
    norm_gain,
    w_bgate,
    w_cgate,
    w_conv_in,
    conv_taps,
    w_query,
    w_key,
    w_value,
    sink_logits,
    conv_out_weight,
    attn_out_weight,
):
    widened = tokens[0].astype(jnp.float32)
    normed = (
        widened
        * lax.rsqrt(jnp.mean(widened * widened, axis=-1, keepdims=True) + epsilon)
        * norm_gain
    ).astype(jnp.bfloat16)
    own, features = normed.shape
    span = WINDOW + 2 * own
    depth, kv = w_key.shape
    width = w_query.shape[1]
    slim = width // m
    chunks = n * m
    bf16 = jnp.bfloat16
    vmem = pl.BlockSpec(memory_space=pltpu.VMEM)
    dma = pltpu.SemaphoreType.DMA
    mixed = pl.pallas_call(
        functools.partial(kernel, n, m),
        out_shape=jax.ShapeDtypeStruct((own, features), bf16),
        in_specs=[vmem] * 10 + [pl.BlockSpec(memory_space=pltpu.SMEM)],
        out_specs=vmem,
        scratch_shapes=[
            pltpu.VMEM((chunks, depth, 2 * kv + 4 * slim), bf16),
            pltpu.VMEM((2, chunks) + conv_out_weight.shape, bf16),
            pltpu.VMEM((m, span, features), bf16),
            pltpu.VMEM((m, span, slim), bf16),
            pltpu.VMEM((m, span, 2 * HEAD), bf16),
            pltpu.VMEM((m, span, slim), bf16),
            pltpu.VMEM((m, 2 * own, slim), bf16),
            pltpu.VMEM((2 * own, width), bf16),
            pltpu.VMEM((2 * own, width), bf16),
            pltpu.VMEM((2 * own, features), jnp.float32),
            pltpu.VMEM((own, features), bf16),
            pltpu.VMEM((own, features), bf16),
            dma((9,)),
            dma((2 * m,)),
            dma((m, 2)),
            dma((2 * m,)),
            dma((m,)),
            dma((6, m)),
            dma((6, m)),
            dma((6, 4, m)),
            dma((6, chunks)),
            dma((6, chunks)),
            dma((6, chunks)),
            dma((6, chunks)),
            dma((2, 4)),
            dma((2, chunks)),
            dma((2, n, m)),
            dma((2, chunks)),
            dma((2, chunks)),
            dma((2, chunks)),
            dma((2, m)),
            dma((2, m)),
            dma((chunks,)),
            dma((chunks,)),
        ],
        compiler_params=pltpu.CompilerParams(
            collective_id=0, has_side_effects=True, vmem_limit_bytes=67_000_000
        ),
    )(
        normed,
        w_key,
        w_value,
        w_query,
        w_cgate,
        w_conv_in,
        w_bgate,
        conv_out_weight,
        attn_out_weight,
        conv_taps,
        sink_logits,
    )
    return mixed[None]


def solution(mesh):
    placed = (
        P(("grp", "fs"), ("sp", "tp"), None),
        P(),
        P(("sp", "fs"), "tp"),
        P(("sp", "fs"), "tp"),
        P(("sp", "fs"), "tp"),
        P(None, "tp"),
        P(("sp", "fs"), "tp"),
        P(("sp", "fs"), "tp"),
        P(("sp", "fs"), "tp"),
        P("tp"),
        P("tp", ("sp", "fs")),
        P("tp", ("sp", "fs")),
    )
    return jax.shard_map(
        functools.partial(local, mesh.shape["sp"], mesh.shape["fs"]),
        mesh=mesh,
        in_specs=placed,
        out_specs=P(("grp", "fs"), ("sp", "tp"), None),
        check_vma=False,
    )
```

profile of v0, /device:TPU:0, one launch (start us, length us, event | category | flops | bytes accessed | tf_op | source)
XLA Modules:
  0.0 228.6 jit_solution(2366558787689978350)
XLA Ops:
  0.0 0.0 copy-start
  0.0 1.6 fusion
  1.6 0.0 copy-done
  1.6 2.0 fusion.2.normed
  3.6 222.7 %shard_map.118 = bf16[256,2048]{1,0:T(8,128)(2,1)} custom-call(bf16[256,2048]{1,0:T(8,128)(2,1)} %fusion.2.normed, bf16[256,128]{1,0:T(8,128)(2,1)} %w_key.1, bf16[256,128]{1,0:T(8,128)(2,1)} %w_value.1, bf16[256,1024]{1,0:T(8,128)(2,1)} %w_query.1, bf16[256,1024]{1,0:T(8,128)(2,1)} %w_cgate.1, bf16[256,1024]{1,0:T(8,128)(2,1)} %w_conv_in.1, ...), custom_call_target="tpu_custom_call" | custom-call | tf_op jit(solution)/shard_map/pallas_call | solution.py:654
  226.3 2.3 %copy.14 = bf16[1,256,2048]{2,1,0:T(8,128)(2,1)} copy(bf16[1,256,2048]{2,1,0:T(8,128)(2,1)} %bitcast.5) | data formatting | bytes 2097152
  (1 shorter events, 0.0 us)
Async XLA Ops:
  0.0 1.6 copy-start
where the time goes:
time: 230 us; the launch traced here: 229 us
  Pallas kernels  223 us (97%)
  other arithmetic  3.58 us (2%)
  local copies, waits for them, and re-layouts  2.31 us (1%)
    pallas_call x1, Pallas kernels, local(): pl.pallas_call(functools.partial(kernel, n, m), out_shape=jax.ShapeDtypeS...  223 us

commit v1 on v0

v1 whole, which is shorter than its diff:
```python
import functools

import jax
import jax.numpy as jnp
from jax import lax
from jax.experimental import pallas as pl
from jax.experimental.pallas import tpu as pltpu
from jax.sharding import PartitionSpec as P

HEAD = 64
WINDOW = 128
TAPS = 3
LANES = 128
HALO = 16
LEAD = 2
MESH = pl.DeviceIdType.MESH

epsilon = 1e-06


def kernel(
    G,
    n,
    m,
    A,
    U,
    tokens,
    gain,
    w_key,
    w_value,
    w_query,
    w_cgate,
    w_conv_in,
    w_bgate,
    conv_weight,
    attn_weight,
    taps,
    sink,
    out,
    kvp,
    kvw,
    wbig,
    w_out,
    rows,
    kv,
    query,
    gate,
    ca,
    precv,
    send1,
    recv1,
    send2,
    recv2,
    fill_sem,
    fillo_sem,
    trade_send,
    trade_recv,
    otrade_send,
    otrade_recv,
    z_send,
    z_recv,
    tx_send,
    ty_send,
    td_send,
    tok_recv,
    hk_send,
    hk_recv,
    hg_send,
    hg_recv,
    d_send,
    d_recv,
    s1_send,
    s1_recv,
    s2_send,
    s2_recv,
):
    big = (w_query, w_cgate, w_conv_in, w_bgate)
    outputs = (conv_weight, attn_weight)
    own, features = tokens.shape
    length = 2 * own
    depth, kvwide = w_key.shape
    width = w_query.shape[1]
    Q = m * G
    slim = width // Q
    heads = slim // HEAD
    per_kv = width // kvwide
    across = conv_weight.shape[1]
    wa = across // A
    gw = features // U
    hw = gw // 2
    ins = 5 * m
    slots = ins + m * A
    bf16 = jnp.bfloat16

    g, s = lax.axis_index("grp"), lax.axis_index("sp")
    f, c = lax.axis_index("fs"), lax.axis_index("tp")
    q = f * G + g

    def loop(low, high, body):
        def step(i, carry):
            body(i)
            return carry

        lax.fori_loop(low, high, step, 0)

    def remote(source, target, send, recv, where):
        return pltpu.make_async_remote_copy(
            source, target, send, recv, device_id=where, device_id_type=MESH
        )

    def to_fs(e):
        return {"fs": lax.rem(f + e, m)}

    def to_grp(y):
        return {"grp": lax.rem(g + y, G)}

    other_core = {"tp": 1 - c}

    def seq(e, y):
        return lax.rem(f + e, m) * G + lax.rem(g + y, G)

    def nth(k):
        return seq(k // G, k % G)

    def kv_head(quarter):
        return quarter * heads // per_kv

    def weights(j, source, chunk):
        return kvw.at[source, chunk] if j == 0 else wbig.at[j - 1, source, chunk]

    def mine_of(j, quarter):
        if j == 0:
            return kvp.at[:, pl.ds(pl.multiple_of(kv_head(quarter) * 2 * HEAD, LANES), 2 * HEAD)]
        return big[j - 1].at[:, pl.ds(pl.multiple_of(quarter * slim, LANES), slim)]

    def out_of(j, a, quarter):
        return outputs[j].at[
            pl.ds(pl.multiple_of(quarter * slim, LANES), slim), pl.ds(a * wa, wa)
        ]

    def fill(j):
        return pltpu.make_async_copy(mine_of(j, q), weights(j, s, f), fill_sem.at[j])

    def fillo(j, a):
        return pltpu.make_async_copy(
            out_of(j, a, q), w_out.at[s, f, a, pl.ds(j * slim, slim)], fillo_sem.at[j, a]
        )

    for h in range(kvwide // HEAD):
        at = pl.ds(h * 2 * HEAD, 2 * HEAD)
        pick = slice(h * HEAD, (h + 1) * HEAD)
        kvp[:, at] = jnp.concatenate([w_key[:, pick], w_value[:, pick]], axis=1)

    for j in range(1, 5):
        fill(j).start()
    for j in range(2):
        for a in range(A):
            fillo(j, a).start()

    barrier = pltpu.get_barrier_semaphore()

    def greet(where):
        pl.semaphore_signal(barrier, inc=1, device_id=where, device_id_type=MESH)

    loop(1, n, lambda d: greet({"sp": lax.rem(s + d, n)}))
    loop(1, m, lambda e: greet(to_fs(e)))
    loop(1, G, lambda y: greet(to_grp(y)))
    greet(other_core)
    fill(0).start()
    pl.semaphore_wait(barrier, n + m + G - 2)

    def trade(j, e):
        t = lax.rem(f + e, m)
        return remote(
            mine_of(j, t * G + g),
            weights(j, s, f),
            trade_send.at[j, e],
            trade_recv.at[j, f],
            {"fs": t},
        )

    def trade_arrival(j, t):
        piece = weights(j, s, t)
        return remote(piece, piece, trade_send.at[j, 0], trade_recv.at[j, t], to_fs(1))

    def otrade(j, a, e):
        t = lax.rem(f + e, m)
        return remote(
            out_of(j, a, t * G + g),
            w_out.at[s, f, a, pl.ds(j * slim, slim)],
            otrade_send.at[j, a, e],
            otrade_recv.at[j, a, f],
            {"fs": t},
        )

    def otrade_arrival(j, a, t):
        piece = w_out.at[s, t, a, pl.ds(j * slim, slim)]
        return remote(piece, piece, otrade_send.at[j, a, 0], otrade_recv.at[j, a, t], to_fs(1))

    def piece(k, source):
        if k < ins:
            return weights(k // m, source, lax.rem(f + k % m, m))
        h, a = (k - ins) // A, (k - ins) % A
        return w_out.at[source, h, a]

    def z_copy(k, source, up, there):
        block = piece(k, source)
        return remote(
            block, block, z_send.at[k, up, source], z_recv.at[k, source], {"sp": there}
        )

    above, below = jnp.minimum(s + 1, n - 1), jnp.maximum(s - 1, 0)

    def own_start(k):
        if k < ins:
            j, h = k // m, k % m
            if h == 0:
                fill(j).wait()
            else:
                trade_arrival(j, lax.rem(f + h, m)).wait_recv()
        else:
            h, a = (k - ins) // A, (k - ins) % A
            for j in range(2):

                @pl.when(f == h)
                def _():
                    fillo(j, a).wait()

                @pl.when(f != h)
                def _():
                    otrade_arrival(j, a, h).wait_recv()

        @pl.when(s < n - 1)
        def _():
            z_copy(k, s, 0, above).start()

        @pl.when(s > 0)
        def _():
            z_copy(k, s, 1, below).start()

    def arrive(k, d):
        low, high = jnp.maximum(s - d, 0), jnp.minimum(s + d, n - 1)

        @pl.when(s - d >= 0)
        def _():
            z_copy(k, low, 0, above).wait_recv()

            @pl.when(s < n - 1)
            def _():
                z_copy(k, low, 0, above).start()

        @pl.when(s + d <= n - 1)
        def _():
            z_copy(k, high, 1, below).wait_recv()

            @pl.when(s > 0)
            def _():
                z_copy(k, high, 1, below).start()

    def arrivals_sent(k):
        @pl.when(s < n - 1)
        def _():
            loop(0, s + 1, lambda source: z_copy(k, source, 0, above).wait_send())

        @pl.when(s > 0)
        def _():
            loop(s, n, lambda source: z_copy(k, source, 1, below).wait_send())

    def tok(i, send, where):
        block = rows.at[i, pl.ds(pl.multiple_of(c * own, LANES), own)]
        return remote(block, block, send, tok_recv.at[i, c], where)

    def tok_x(e, y):
        return tok(seq(0, y), tx_send.at[e, y], to_fs(e))

    def tok_y(e, y):
        return tok(seq(e, 0), ty_send.at[e, y], to_grp(y))

    def tok_d(i):
        return tok(i, td_send.at[i], other_core)

    def tok_here(i, half):
        block = rows.at[i, pl.ds(pl.multiple_of(half * own, LANES), own)]
        return remote(block, block, td_send.at[i], tok_recv.at[i, half], other_core)

    def normalize():
        scale = gain[...]
        step = 16

        def body(t):
            at = pl.multiple_of(t * step, step)
            wide = tokens[pl.ds(at, step), :].astype(jnp.float32)
            norm = lax.rsqrt(jnp.mean(wide * wide, axis=-1, keepdims=True) + epsilon)
            rows[q, pl.ds(pl.multiple_of(c * own + at, step), step), :] = (
                wide * norm * scale
            ).astype(bf16)

        loop(0, own // step, body)

    def tokens_first():
        @pl.when(c == 0)
        def _():
            for e in range(1, m):
                tok_x(e, 0).start()
            for y in range(1, G):
                tok_y(0, y).start()

        @pl.when(c == 1)
        def _():
            for y in range(1, G):
                tok_y(0, y).start()
            for e in range(1, m):
                tok_x(e, 0).start()

        tok_d(q).start()

    def tokens_relay():
        @pl.when(c == 0)
        def _():
            for e in range(1, m):
                i = seq(e, 0)
                tok_here(i, c).wait_recv()
                for y in range(1, G):
                    tok_y(e, y).start()
                tok_d(i).start()

        @pl.when(c == 1)
        def _():
            for y in range(1, G):
                i = seq(0, y)
                tok_here(i, c).wait_recv()
                for e in range(1, m):
                    tok_x(e, y).start()
                tok_d(i).start()

    def tokens_near():
        def here(i):
            tok_here(i, c).wait_recv()
            tok_d(i).start()

        @pl.when(c == 0)
        def _():
            for y in range(1, G):
                here(seq(0, y))

        @pl.when(c == 1)
        def _():
            for e in range(1, m):
                here(seq(e, 0))

    def tokens_ready(k):
        i = nth(k)

        @pl.when((k // G > 0) & (k % G > 0))
        def _():
            tok_here(i, c).wait_recv()
            tok_d(i).start()

        tok_here(i, 1 - c).wait_recv()

    def tokens_sent():
        @pl.when(c == 0)
        def _():
            for e in range(1, m):
                tok_x(e, 0).wait_send()
            for e in range(m):
                for y in range(1, G):
                    tok_y(e, y).wait_send()

        @pl.when(c == 1)
        def _():
            for y in range(1, G):
                tok_y(0, y).wait_send()
            for e in range(1, m):
                for y in range(G):
                    tok_x(e, y).wait_send()

        loop(0, Q, lambda i: tok_d(i).wait_send())

    def halo_kv(i):
        return remote(
            kv.at[i, pl.ds(length, WINDOW)],
            kv.at[i, pl.ds(0, WINDOW)],
            hk_send.at[i],
            hk_recv.at[i],
            {"sp": above},
        )

    def halo_gate(i):
        return remote(
            gate.at[i, pl.ds(length, HALO)],
            gate.at[i, pl.ds(0, HALO)],
            hg_send.at[i],
            hg_recv.at[i],
            {"sp": above},
        )

    def project(j, i):
        block = kvw[...] if j == 0 else wbig[j - 1]
        block = block.reshape(n * m * depth, block.shape[-1])
        return jnp.dot(rows[i], block, preferred_element_type=jnp.float32)

    def do_keys(i):
        kv[i, pl.ds(WINDOW, length), :] = project(0, i).astype(bf16)

        @pl.when(s < n - 1)
        def _():
            halo_kv(i).start()

    def do_query(i):
        query[i] = project(1, i).astype(bf16)

    def do_gate(i):
        gate[i, pl.ds(HALO, length), :] = project(2, i).astype(bf16)

    def do_gated(i):
        values = project(3, i).astype(bf16).astype(jnp.float32)
        here = pl.ds(HALO, length)
        gate[i, here, :] = (gate[i, here, :].astype(jnp.float32) * values).astype(bf16)

        @pl.when(s < n - 1)
        def _():
            halo_gate(i).start()

    def do_conv(i):
        @pl.when(s > 0)
        def _():
            halo_gate(i).wait_recv()

        outer = project(4, i).astype(bf16).astype(jnp.float32)
        gated = gate[i].astype(jnp.float32)
        there = pl.ds(pl.multiple_of(q * slim, LANES), slim)
        mixed = None
        for which in range(TAPS):
            tap = taps[pl.ds(which, 1), there].astype(jnp.float32)
            low = HALO - TAPS + 1 + which
            term = tap * gated[low : low + length]
            mixed = term if mixed is None else mixed + term
        ca[i, :, pl.ds(0, slim)] = (outer * mixed).astype(bf16)

    pairs = 2 * HEAD
    blocks = length // WINDOW
    place_q = lax.broadcasted_iota(jnp.int32, (WINDOW, 2 * WINDOW), 0)
    place_k = lax.broadcasted_iota(jnp.int32, (WINDOW, 2 * WINDOW), 1)
    banded = (place_k > place_q) & (place_k <= place_q + WINDOW)

    def do_attention(i, b):
        row = pl.multiple_of(b * WINDOW, WINDOW)
        band = kv[i, pl.ds(row, 2 * WINDOW), :]
        key, value = band[:, :HEAD], band[:, HEAD:]
        least = jnp.where((s == 0) & (b == 0), WINDOW, 0)
        allowed = banded & (place_k >= least)
        for p in range(heads // 2):
            at = p * pairs
            both = query[i, pl.ds(row, WINDOW), pl.ds(at, pairs)]
            results = []
            for half in range(2):
                one = both[:, half * HEAD : (half + 1) * HEAD]
                scores = lax.dot_general(
                    one, key, (((1,), (1,)), ((), ())), preferred_element_type=jnp.float32
                ) * (1.0 / HEAD**0.5)
                scores = jnp.where(allowed, scores, -jnp.inf)
                logit = sink[q * heads + 2 * p + half]
                peak = jnp.maximum(jnp.max(scores, axis=-1, keepdims=True), logit)
                powers = jnp.exp(scores - peak)
                norm = jnp.sum(powers, axis=-1, keepdims=True) + jnp.exp(logit - peak)
                probs = (powers / norm).astype(bf16)
                results.append(jnp.dot(probs, value, preferred_element_type=jnp.float32))
            ca[i, pl.ds(row, WINDOW), pl.ds(slim + at, pairs)] = jnp.concatenate(
                results, axis=1
            ).astype(bf16)

    def columns(u, v=0, count=gw):
        return pl.ds(u * gw + v * hw, count)

    def half_rows(half):
        return pl.ds(pl.multiple_of(half * own, LANES), own)

    def core_copy(u, i):
        return remote(
            rows.at[i, half_rows(1 - c), columns(u)],
            precv.at[u, i],
            d_send.at[u, i],
            d_recv.at[u, i],
            other_core,
        )

    def chunk_of(u, t):
        if U == 1:
            return w_out[t // m, t % m, 0]
        return w_out[t, u // A, u % A]

    def do_out(u, i):
        per = max(1, min(2 * LANES, gw) // wa)

        for t in range(gw // (per * wa)):
            block = jnp.concatenate([chunk_of(u, t * per + k) for k in range(per)], axis=1)
            rows[i, :, pl.ds(u * gw + t * per * wa, per * wa)] = jnp.dot(
                ca[i], block, preferred_element_type=jnp.float32
            ).astype(bf16)
        core_copy(u, i).start()

    counts = ((G, m), (m, G))

    def ordered(v, first, second):
        return seq(second, first) if v == 0 else seq(first, second)

    def to_first(v, e):
        return to_grp(e) if v == 0 else to_fs(e)

    def to_second(v, e):
        return to_fs(e) if v == 0 else to_grp(e)

    def first_copy(u, v, e):
        n2 = counts[v][1]
        which = pl.ds((e - 1) * n2, n2)
        return remote(
            send1.at[u, v, which],
            recv1.at[u, v, which],
            s1_send.at[u, v, e - 1],
            s1_recv.at[u, v, e - 1],
            to_first(v, e),
        )

    def second_copy(u, v, e):
        return remote(
            send2.at[u, v, e - 1],
            recv2.at[u, v, e - 1],
            s2_send.at[u, v, e - 1],
            s2_recv.at[u, v, e - 1],
            to_second(v, e),
        )

    def both_cores(u, v, i):
        here = rows[i, half_rows(c), columns(u, v, hw)].astype(jnp.float32)
        return here + precv[u, i, :, pl.ds(v * hw, hw)].astype(jnp.float32)

    def stage_one(u):
        loop(0, Q, lambda i: core_copy(u, i).wait_recv())
        for v in range(2):
            n1, n2 = counts[v]
            for e in range(1, n1):
                for i2 in range(n2):
                    send1[u, v, (e - 1) * n2 + i2] = both_cores(u, v, ordered(v, e, i2)).astype(bf16)
                first_copy(u, v, e).start()

    def with_first(u, v, i2):
        n1, n2 = counts[v]
        value = both_cores(u, v, ordered(v, 0, i2))
        for e in range(1, n1):
            value = value + recv1[u, v, (e - 1) * n2 + i2].astype(jnp.float32)
        return value

    def stage_two(u):
        for v in range(2):
            n1, n2 = counts[v]
            for e in range(1, n1):
                first_copy(u, v, e).wait_recv()
            for i2 in range(1, n2):
                send2[u, v, i2 - 1] = with_first(u, v, i2).astype(bf16)
                second_copy(u, v, i2).start()

    def stage_three(u):
        for v in range(2):
            value = with_first(u, v, 0)
            for i2 in range(1, counts[v][1]):
                second_copy(u, v, i2).wait_recv()
                value = value + recv2[u, v, i2 - 1].astype(jnp.float32)
            value = value.astype(bf16)
            if U == 1:
                out[:, pl.ds(v * hw, hw)] = value
            else:
                for k in range(hw // wa):
                    source = v * (hw // wa) + k
                    chunk = source * m + u // A
                    at = chunk * across + (u % A) * wa
                    out[:, pl.ds(at, wa)] = value[:, k * wa : (k + 1) * wa]

    for j in range(5):
        loop(1, m, lambda e: trade(j, e).start())
        if j == 0:
            own_start(0)
    for k in range(1, LEAD):
        own_start(k)
    normalize()
    tokens_first()
    for j in range(2):
        for a in range(A):
            loop(1, m, lambda e: otrade(j, a, e).start())

    @pl.when(s == 0)
    def _():
        kv[:, pl.ds(0, WINDOW), :] = jnp.zeros((Q, WINDOW, 2 * HEAD), bf16)
        gate[:, pl.ds(0, HALO), :] = jnp.zeros((Q, HALO, slim), bf16)

    def attend(h, r):
        unit = h * 2 * G + r
        k, low = unit // 2, (unit % 2) * (blocks // 2)
        i = nth(k)

        @pl.when((s > 0) & (unit % 2 == 0))
        def _():
            halo_kv(i).wait_recv()

        loop(0, blocks // 2, lambda b: do_attention(i, low + b))

    def task(k, r):
        if k == 3 * m - 1:
            tokens_ready(r)
            do_keys(nth(r))
            do_query(nth(r))
        elif 3 * m <= k < 4 * m:
            attend(k - 3 * m, r)
        elif k == 4 * m:
            do_gate(nth(r))
        elif k == 4 * m + 1:
            do_gated(nth(r))
        elif k == ins:
            do_conv(nth(r))
        elif U > 1 and k > ins:
            do_out(k - ins - 1, nth(r))

    busy = set([3 * m - 1] + list(range(3 * m, 4 * m + 2)) + list(range(ins, slots)))
    for k in range(slots):
        if k + LEAD < slots:
            own_start(k + LEAD)
        if k == ins + 1:
            tokens_sent()
        turns = (2 * G if 3 * m <= k < 4 * m else Q) if k in busy else n - 1
        each = -(-(n - 1) // turns)

        def body(r):
            for dd in range(each):
                d = r * each + dd + 1

                @pl.when(d < n)
                def _():
                    arrive(k, d)

            task(k, r)

        loop(0, turns, body)
        if k == 2 * m - 1:
            tokens_relay()
        if k == 3 * m - 2:
            tokens_near()
        if U > 1 and k > ins:
            u = k - ins - 1
            if u >= 2:
                stage_three(u - 2)
            if u >= 1:
                stage_two(u - 1)
            stage_one(u)
    loop(0, Q, lambda r: do_out(U - 1, nth(r)))
    if U > 1:
        stage_two(U - 2)
    stage_one(U - 1)
    if U > 2:
        stage_three(U - 3)
    if U > 1:
        stage_three(U - 2)
    stage_two(U - 1)
    stage_three(U - 1)

    for j in range(5):
        loop(1, m, lambda e: trade(j, e).wait_send())
    for j in range(2):
        for a in range(A):
            loop(1, m, lambda e: otrade(j, a, e).wait_send())
    for k in range(slots):
        arrivals_sent(k)

    @pl.when(s < n - 1)
    def _():
        loop(0, Q, lambda i: halo_kv(i).wait_send())
        loop(0, Q, lambda i: halo_gate(i).wait_send())

    for u in range(U):
        loop(0, Q, lambda i: core_copy(u, i).wait_send())
        for v in range(2):
            for e in range(1, counts[v][0]):
                first_copy(u, v, e).wait_send()
            for e in range(1, counts[v][1]):
                second_copy(u, v, e).wait_send()


def local(
    G,
    n,
    m,
    tokens,
    norm_gain,
    w_bgate,
    w_cgate,
    w_conv_in,
    conv_taps,
    w_query,
    w_key,
    w_value,
    sink_logits,
    conv_out_weight,
    attn_out_weight,
):
    own, features = tokens.shape[1:]
    length = 2 * own
    depth, kvwide = w_key.shape
    width = w_query.shape[1]
    across = conv_out_weight.shape[1]
    Q = m * G
    slim = width // Q
    A = 2 if across % (2 * LANES) == 0 else 1
    U = m * A if across % LANES == 0 else 1
    wa = across // A
    gw = features // U
    slots = 5 * m + m * A
    n1, n2 = max(m, G) - 1, max(m, G)
    cnt = max((G - 1) * m, (m - 1) * G)
    bf16 = jnp.bfloat16
    vmem = pl.BlockSpec(memory_space=pltpu.VMEM)
    dma = pltpu.SemaphoreType.DMA
    mixed = pl.pallas_call(
        functools.partial(kernel, G, n, m, A, U),
        out_shape=jax.ShapeDtypeStruct((own, features), bf16),
        in_specs=[vmem] * 11 + [pl.BlockSpec(memory_space=pltpu.SMEM)],
        out_specs=vmem,
        scratch_shapes=[
            pltpu.VMEM((depth, 2 * kvwide), bf16),
            pltpu.VMEM((n, m, depth, 2 * HEAD), bf16),
            pltpu.VMEM((4, n, m, depth, slim), bf16),
            pltpu.VMEM((n, m, A, 2 * slim, wa), bf16),
            pltpu.VMEM((Q, length, features), bf16),
            pltpu.VMEM((Q, WINDOW + length, 2 * HEAD), bf16),
            pltpu.VMEM((Q, length, slim), bf16),
            pltpu.VMEM((Q, HALO + length, slim), bf16),
            pltpu.VMEM((Q, length, 2 * slim), bf16),
            pltpu.VMEM((U, Q, own, gw), bf16),
            pltpu.VMEM((U, 2, cnt, own, gw // 2), bf16),
            pltpu.VMEM((U, 2, cnt, own, gw // 2), bf16),
            pltpu.VMEM((U, 2, n1, own, gw // 2), bf16),
            pltpu.VMEM((U, 2, n1, own, gw // 2), bf16),
            dma((5,)),
            dma((2, A)),
            dma((5, m)),
            dma((5, m)),
            dma((2, A, m)),
            dma((2, A, m)),
            dma((slots, 2, n)),
            dma((slots, n)),
            dma((m, G)),
            dma((m, G)),
            dma((Q,)),
            dma((Q, 2)),
            dma((Q,)),
            dma((Q,)),
            dma((Q,)),
            dma((Q,)),
            dma((U, Q)),
            dma((U, Q)),
            dma((U, 2, n1)),
            dma((U, 2, n1)),
            dma((U, 2, n1)),
            dma((U, 2, n1)),
        ],
        compiler_params=pltpu.CompilerParams(
            collective_id=0, has_side_effects=True, vmem_limit_bytes=67_000_000
        ),
    )(
        tokens[0],
        norm_gain[None],
        w_key,
        w_value,
        w_query,
        w_cgate,
        w_conv_in,
        w_bgate,
        conv_out_weight,
        attn_out_weight,
        conv_taps,
        sink_logits,
    )
    return mixed[None]


def solution(mesh):
    placed = (
        P(("grp", "fs"), ("sp", "tp"), None),
        P(),
        P(("sp", "fs"), "tp"),
        P(("sp", "fs"), "tp"),
        P(("sp", "fs"), "tp"),
        P(None, "tp"),
        P(("sp", "fs"), "tp"),
        P(("sp", "fs"), "tp"),
        P(("sp", "fs"), "tp"),
        P("tp"),
        P("tp", ("sp", "fs")),
        P("tp", ("sp", "fs")),
    )
    return jax.shard_map(
        functools.partial(local, mesh.shape["grp"], mesh.shape["sp"], mesh.shape["fs"]),
        mesh=mesh,
        in_specs=placed,
        out_specs=P(("grp", "fs"), ("sp", "tp"), None),
        check_vma=False,
    )
```

time: 230 us -> 180 us (0.78)
  Pallas kernels: 223 us -> 178 us
  other arithmetic: 3.58 us -> 0 us
    pallas_call x1, Pallas kernels: 223 us -> 178 us  [local(): pl.pallas_call(functools.partial(kernel, G, n, m, A, U), out_shape=jax.Sh...]
where the time goes in v1:
time: 180 us
  Pallas kernels  178 us (99%)
  local copies, waits for them, and re-layouts  2.3 us (1%)
    pallas_call x1, Pallas kernels, local(): pl.pallas_call(functools.partial(kernel, G, n, m, A, U), out_shape=jax.Sh...  178 us

profile of v1, /device:TPU:0, one launch (start us, length us, event | category | flops | bytes accessed | tf_op | source)
XLA Modules:
  0.0 180.2 jit_solution(1613742564151285122)
XLA Ops:
  0.0 177.9 %shard_map.118 = bf16[256,2048]{1,0:T(8,128)(2,1)} custom-call(bf16[256,2048]{1,0:T(8,128)(2,1)} %bitcast.4, f32[1,2048]{1,0:T(1,128)} %bitcast.5, bf16[256,128]{1,0:T(8,128)(2,1)} %w_key.1, bf16[256,128]{1,0:T(8,128)(2,1)} %w_value.1, bf16[256,1024]{1,0:T(8,128)(2,1)} %w_query.1, bf16[256,1024]{1,0:T(8,128)(2,1)} %w_cgate.1, bf16[256,1024]{1,0:T(8,128)(2,1)} %w_conv_in.1, ...), custom_call_target="tpu_custom_call" | custom-call | tf_op jit(solution)/shard_map/pallas_call | solution.py:721
  177.9 2.3 %copy.14 = bf16[1,256,2048]{2,1,0:T(8,128)(2,1)} copy(bf16[1,256,2048]{2,1,0:T(8,128)(2,1)} %bitcast.3) | data formatting | bytes 2097152

commit v2 on v1

--- a/solution.py
+++ b/solution.py
@@ -12,8 +12,15 @@
 TAPS = 3
 LANES = 128
 HALO = 16
-LEAD = 2
+LEAD = 6
 MESH = pl.DeviceIdType.MESH
+
+KEYS = (2, 7, 10, 14)
+QUERY = (6, 8, 11, 15)
+ATTEND = (7, 11, 15, 19)
+GATE = (12, 13, 16, 17)
+GATED = (18, 19, 20, 21)
+RELAY = (4, 5, 8, 13)
 
 epsilon = 1e-06
 
@@ -86,8 +93,7 @@
     per_kv = width // kvwide
     across = conv_weight.shape[1]
     wa = across // A
-    gw = features // U
-    hw = gw // 2
+    hr = own // 2
     ins = 5 * m
     slots = ins + m * A
     bf16 = jnp.bfloat16
@@ -314,49 +320,35 @@
 
         tok_d(q).start()
 
-    def tokens_relay():
-        @pl.when(c == 0)
-        def _():
-            for e in range(1, m):
-                i = seq(e, 0)
-                tok_here(i, c).wait_recv()
-                for y in range(1, G):
-                    tok_y(e, y).start()
-                tok_d(i).start()
-
-        @pl.when(c == 1)
-        def _():
-            for y in range(1, G):
-                i = seq(0, y)
-                tok_here(i, c).wait_recv()
-                for e in range(1, m):
-                    tok_x(e, y).start()
-                tok_d(i).start()
-
-    def tokens_near():
-        def here(i):
-            tok_here(i, c).wait_recv()
-            tok_d(i).start()
-
-        @pl.when(c == 0)
-        def _():
-            for y in range(1, G):
-                here(seq(0, y))
-
-        @pl.when(c == 1)
-        def _():
-            for e in range(1, m):
-                here(seq(e, 0))
-
-    def tokens_ready(k):
-        i = nth(k)
-
-        @pl.when((k // G > 0) & (k % G > 0))
-        def _():
-            tok_here(i, c).wait_recv()
-            tok_d(i).start()
-
-        tok_here(i, 1 - c).wait_recv()
+    def tokens_relay(core):
+        @pl.when(c == core)
+        def _():
+            for k in range(1, Q):
+                e, y = k // G, k % G
+                if core == 0 and y == 0:
+                    tokens_on(nth(k))
+                    for far in range(1, G):
+                        tok_y(e, far).start()
+                if core == 1 and e == 0:
+                    tokens_on(nth(k))
+                    for far in range(1, m):
+                        tok_x(far, y).start()
+
+    def tokens_on(i):
+        tok_here(i, c).wait_recv()
+        tok_d(i).start()
+
+    def tokens_direct(core):
+        @pl.when(c == core)
+        def _():
+            for k in range(1, Q):
+                if (k // G == 0) == (core == 0) and (k // G) * (k % G) == 0:
+                    tokens_on(nth(k))
+
+    def tokens_far():
+        for k in range(1, Q):
+            if (k // G) * (k % G) > 0:
+                tokens_on(nth(k))
 
     def tokens_sent():
         @pl.when(c == 0)
@@ -401,6 +393,7 @@
         return jnp.dot(rows[i], block, preferred_element_type=jnp.float32)
 
     def do_keys(i):
+        tok_here(i, 1 - c).wait_recv()
         kv[i, pl.ds(WINDOW, length), :] = project(0, i).astype(bf16)
 
         @pl.when(s < n - 1)
@@ -470,8 +463,22 @@
                 results, axis=1
             ).astype(bf16)
 
-    def columns(u, v=0, count=gw):
-        return pl.ds(u * gw + v * hw, count)
+    def other_plane(d):
+        return lax.rem(jnp.where(2 * s >= n, s - d + n, s + d), n)
+
+    def chunks_of(u):
+        if U == 1:
+            return [(t // m, t % m, 0) for t in range(n * m)]
+        if u == 0:
+            return [(s, h, a) for h in range(m) for a in range(A)]
+        return [(other_plane(d), (u - 1) // A, (u - 1) % A) for d in range(1, n)]
+
+    lists = [chunks_of(u) for u in range(U)]
+    sizes = [len(chunks) * wa for chunks in lists]
+    firsts = [sum(sizes[:u]) for u in range(U)]
+
+    def columns(u):
+        return pl.ds(firsts[u], sizes[u])
 
     def half_rows(half):
         return pl.ds(pl.multiple_of(half * own, LANES), own)
@@ -479,23 +486,18 @@
     def core_copy(u, i):
         return remote(
             rows.at[i, half_rows(1 - c), columns(u)],
-            precv.at[u, i],
+            precv.at[i, :, columns(u)],
             d_send.at[u, i],
             d_recv.at[u, i],
             other_core,
         )
 
-    def chunk_of(u, t):
-        if U == 1:
-            return w_out[t // m, t % m, 0]
-        return w_out[t, u // A, u % A]
-
     def do_out(u, i):
-        per = max(1, min(2 * LANES, gw) // wa)
-
-        for t in range(gw // (per * wa)):
-            block = jnp.concatenate([chunk_of(u, t * per + k) for k in range(per)], axis=1)
-            rows[i, :, pl.ds(u * gw + t * per * wa, per * wa)] = jnp.dot(
+        per = max(1, 2 * LANES // wa)
+        for t in range(0, len(lists[u]), per):
+            some = lists[u][t : t + per]
+            block = jnp.concatenate([w_out[p, h, a] for p, h, a in some], axis=1)
+            rows[i, :, pl.ds(firsts[u] + t * wa, len(some) * wa)] = jnp.dot(
                 ca[i], block, preferred_element_type=jnp.float32
             ).astype(bf16)
         core_copy(u, i).start()
@@ -515,8 +517,8 @@
         n2 = counts[v][1]
         which = pl.ds((e - 1) * n2, n2)
         return remote(
-            send1.at[u, v, which],
-            recv1.at[u, v, which],
+            send1.at[v, which, :, columns(u)],
+            recv1.at[v, which, :, columns(u)],
             s1_send.at[u, v, e - 1],
             s1_recv.at[u, v, e - 1],
             to_first(v, e),
@@ -524,16 +526,17 @@
 
     def second_copy(u, v, e):
         return remote(
-            send2.at[u, v, e - 1],
-            recv2.at[u, v, e - 1],
+            send2.at[v, e - 1, :, columns(u)],
+            recv2.at[v, e - 1, :, columns(u)],
             s2_send.at[u, v, e - 1],
             s2_recv.at[u, v, e - 1],
             to_second(v, e),
         )
 
     def both_cores(u, v, i):
-        here = rows[i, half_rows(c), columns(u, v, hw)].astype(jnp.float32)
-        return here + precv[u, i, :, pl.ds(v * hw, hw)].astype(jnp.float32)
+        at = pl.ds(pl.multiple_of(c * own + v * hr, HALO), hr)
+        here = rows[i, at, columns(u)].astype(jnp.float32)
+        return here + precv[i, pl.ds(v * hr, hr), columns(u)].astype(jnp.float32)
 
     def stage_one(u):
         loop(0, Q, lambda i: core_copy(u, i).wait_recv())
@@ -541,14 +544,15 @@
             n1, n2 = counts[v]
             for e in range(1, n1):
                 for i2 in range(n2):
-                    send1[u, v, (e - 1) * n2 + i2] = both_cores(u, v, ordered(v, e, i2)).astype(bf16)
+                    value = both_cores(u, v, ordered(v, e, i2))
+                    send1[v, (e - 1) * n2 + i2, :, columns(u)] = value.astype(bf16)
                 first_copy(u, v, e).start()
 
     def with_first(u, v, i2):
         n1, n2 = counts[v]
         value = both_cores(u, v, ordered(v, 0, i2))
         for e in range(1, n1):
-            value = value + recv1[u, v, (e - 1) * n2 + i2].astype(jnp.float32)
+            value = value + recv1[v, (e - 1) * n2 + i2, :, columns(u)].astype(jnp.float32)
         return value
 
     def stage_two(u):
@@ -557,7 +561,7 @@
             for e in range(1, n1):
                 first_copy(u, v, e).wait_recv()
             for i2 in range(1, n2):
-                send2[u, v, i2 - 1] = with_first(u, v, i2).astype(bf16)
+                send2[v, i2 - 1, :, columns(u)] = with_first(u, v, i2).astype(bf16)
                 second_copy(u, v, i2).start()
 
     def stage_three(u):
@@ -565,102 +569,133 @@
             value = with_first(u, v, 0)
             for i2 in range(1, counts[v][1]):
                 second_copy(u, v, i2).wait_recv()
-                value = value + recv2[u, v, i2 - 1].astype(jnp.float32)
+                value = value + recv2[v, i2 - 1, :, columns(u)].astype(jnp.float32)
             value = value.astype(bf16)
             if U == 1:
-                out[:, pl.ds(v * hw, hw)] = value
+                out[pl.ds(v * hr, hr), :] = value
             else:
-                for k in range(hw // wa):
-                    source = v * (hw // wa) + k
-                    chunk = source * m + u // A
-                    at = chunk * across + (u % A) * wa
-                    out[:, pl.ds(at, wa)] = value[:, k * wa : (k + 1) * wa]
+                for k, (p, h, a) in enumerate(lists[u]):
+                    at = pl.multiple_of((p * m + h) * across + a * wa, LANES)
+                    out[pl.ds(v * hr, hr), pl.ds(at, wa)] = value[:, k * wa : (k + 1) * wa]
 
     for j in range(5):
         loop(1, m, lambda e: trade(j, e).start())
         if j == 0:
             own_start(0)
-    for k in range(1, LEAD):
+    for k in range(m, LEAD, m):
         own_start(k)
     normalize()
     tokens_first()
     for j in range(2):
         for a in range(A):
             loop(1, m, lambda e: otrade(j, a, e).start())
+    for k in range(LEAD):
+        if k % m > 0:
+            own_start(k)
 
     @pl.when(s == 0)
     def _():
         kv[:, pl.ds(0, WINDOW), :] = jnp.zeros((Q, WINDOW, 2 * HEAD), bf16)
         gate[:, pl.ds(0, HALO), :] = jnp.zeros((Q, HALO, slim), bf16)
 
-    def attend(h, r):
-        unit = h * 2 * G + r
-        k, low = unit // 2, (unit % 2) * (blocks // 2)
-        i = nth(k)
-
-        @pl.when((s > 0) & (unit % 2 == 0))
+    def attend(unit):
+        i = nth(unit // blocks)
+
+        @pl.when((s > 0) & (unit % blocks == 0))
         def _():
             halo_kv(i).wait_recv()
 
-        loop(0, blocks // 2, lambda b: do_attention(i, low + b))
-
-    def task(k, r):
-        if k == 3 * m - 1:
-            tokens_ready(r)
-            do_keys(nth(r))
-            do_query(nth(r))
-        elif 3 * m <= k < 4 * m:
-            attend(k - 3 * m, r)
-        elif k == 4 * m:
-            do_gate(nth(r))
-        elif k == 4 * m + 1:
-            do_gated(nth(r))
-        elif k == ins:
-            do_conv(nth(r))
-        elif U > 1 and k > ins:
-            do_out(k - ins - 1, nth(r))
-
-    busy = set([3 * m - 1] + list(range(3 * m, 4 * m + 2)) + list(range(ins, slots)))
+        do_attention(i, unit % blocks)
+
+    span = m * (n - 1)
+
+    def place(base):
+        return base * span // 6
+
+    kinds = [0 if k == 0 else 1 if k // G == 0 else 2 if k % G == 0 else 3 for k in range(Q)]
+    again = [kinds[:k].count(kinds[k]) for k in range(Q)]
+
+    def times(bases):
+        return [(place(bases[kinds[k]]) + again[k], k) for k in range(Q)]
+
+    plan = [
+        (do_keys, True, times(KEYS)),
+        (do_query, True, times(QUERY)),
+        (do_gate, True, times(GATE)),
+        (do_gated, True, times(GATED)),
+        (
+            attend,
+            False,
+            [
+                (place(ATTEND[kinds[k]] + b) + again[k], k * blocks + b)
+                for k in range(Q)
+                for b in range(blocks)
+            ],
+        ),
+    ]
+    relays = [
+        (place(RELAY[0]), functools.partial(tokens_relay, 1)),
+        (place(RELAY[1]), functools.partial(tokens_direct, 0)),
+        (place(RELAY[2]), functools.partial(tokens_relay, 0)),
+        (place(RELAY[2]), functools.partial(tokens_direct, 1)),
+        (place(RELAY[3]), tokens_far),
+    ]
+
+    def tasks(first, count, r):
+        for when, run in relays:
+            if first <= when < first + count:
+                pl.when(r == when - first)(run)
+        for run, whole, entries in plan:
+            here = [(t - first, k) for t, k in entries if first <= t < first + count]
+            if here:
+                hit, index = False, 0
+                for t, k in here:
+                    hit = (r == t) | hit
+                    index = jnp.where(r == t, k, index)
+                pl.when(hit)(functools.partial(run, nth(index) if whole else index))
+
+    stages = {"o": lambda u: loop(0, Q, lambda r: do_out(u, nth(r)))}
+    stages.update({"1": stage_one, "2": stage_two, "3": stage_three})
+    events = {}
+    last = U - 1
+    if U > 1:
+        for u in range(U):
+            if u > 0:
+                events.setdefault((ins + u - 1, n - 2), []).append(("o", u))
+            for name, k, r in (("1", ins + u, 1 if u == 0 else 0), ("2", ins + u + 1, 1), ("3", ins + u + 2, 1)):
+                if k < slots:
+                    events.setdefault((k, min(r, n - 2)), []).append((name, u))
+
     for k in range(slots):
         if k + LEAD < slots:
             own_start(k + LEAD)
-        if k == ins + 1:
+        if k == ins and U == 1:
+            loop(0, Q, lambda r: do_conv(nth(r)))
             tokens_sent()
-        turns = (2 * G if 3 * m <= k < 4 * m else Q) if k in busy else n - 1
-        each = -(-(n - 1) // turns)
+        if k >= ins and U > 1:
+            for r in range(n - 1):
+                if k == ins and r == 0:
+                    loop(0, Q // 2, lambda i: do_conv(nth(i)))
+                if k == ins and r == 1:
+                    loop(Q // 2, Q, lambda i: do_conv(nth(i)))
+                    tokens_sent()
+                    stages["o"](0)
+                arrive(k, r + 1)
+                for name, u in sorted(events.get((k, r), []), key=lambda event: event[0]):
+                    stages[name](u)
+            continue
 
         def body(r):
-            for dd in range(each):
-                d = r * each + dd + 1
-
-                @pl.when(d < n)
-                def _():
-                    arrive(k, d)
-
-            task(k, r)
-
-        loop(0, turns, body)
-        if k == 2 * m - 1:
-            tokens_relay()
-        if k == 3 * m - 2:
-            tokens_near()
-        if U > 1 and k > ins:
-            u = k - ins - 1
-            if u >= 2:
-                stage_three(u - 2)
-            if u >= 1:
-                stage_two(u - 1)
-            stage_one(u)
-    loop(0, Q, lambda r: do_out(U - 1, nth(r)))
-    if U > 1:
-        stage_two(U - 2)
-    stage_one(U - 1)
-    if U > 2:
-        stage_three(U - 3)
-    if U > 1:
-        stage_three(U - 2)
-    stage_two(U - 1)
-    stage_three(U - 1)
+            arrive(k, r + 1)
+            if m <= k < ins:
+                tasks((k - m) * (n - 1), n - 1, r)
+
+        loop(0, n - 1, body)
+    if U == 1:
+        stages["o"](0)
+    for name, u in (("1", last), ("2", last - 1), ("3", last - 2), ("3", last - 1), ("2", last), ("3", last)):
+        if u >= 0:
+            stages[name](u)
 
     for j in range(5):
         loop(1, m, lambda e: trade(j, e).wait_send())
@@ -709,11 +744,10 @@
     Q = m * G
     slim = width // Q
     A = 2 if across % (2 * LANES) == 0 else 1
-    U = m * A if across % LANES == 0 else 1
+    U = m * A + 1 if across % LANES == 0 else 1
     wa = across // A
-    gw = features // U
     slots = 5 * m + m * A
-    n1, n2 = max(m, G) - 1, max(m, G)
+    n1 = max(m, G) - 1
     cnt = max((G - 1) * m, (m - 1) * G)
     bf16 = jnp.bfloat16
     vmem = pl.BlockSpec(memory_space=pltpu.VMEM)
@@ -733,11 +767,11 @@
             pltpu.VMEM((Q, length, slim), bf16),
             pltpu.VMEM((Q, HALO + length, slim), bf16),
             pltpu.VMEM((Q, length, 2 * slim), bf16),
-            pltpu.VMEM((U, Q, own, gw), bf16),
-            pltpu.VMEM((U, 2, cnt, own, gw // 2), bf16),
-            pltpu.VMEM((U, 2, cnt, own, gw // 2), bf16),
-            pltpu.VMEM((U, 2, n1, own, gw // 2), bf16),
-            pltpu.VMEM((U, 2, n1, own, gw // 2), bf16),
+            pltpu.VMEM((Q, own, features), bf16),
+            pltpu.VMEM((2, cnt, own // 2, features), bf16),
+            pltpu.VMEM((2, cnt, own // 2, features), bf16),
+            pltpu.VMEM((2, n1, own // 2, features), bf16),
+            pltpu.VMEM((2, n1, own // 2, features), bf16),
             dma((5,)),
             dma((2, A)),
             dma((5, m)),

time: 180 us -> 155 us (0.86)
  Pallas kernels: 178 us -> 153 us
    pallas_call x1, Pallas kernels: 178 us -> 153 us  [local(): pl.pallas_call(functools.partial(kernel, G, n, m, A, U), out_shape=jax.Sh...]
where the time goes in v2:
time: 155 us
  Pallas kernels  153 us (99%)
  local copies, waits for them, and re-layouts  2.3 us (1%)
    pallas_call x1, Pallas kernels, local(): pl.pallas_call(functools.partial(kernel, G, n, m, A, U), out_shape=jax.Sh...  153 us

profile of v2, /device:TPU:0, one launch (start us, length us, event | category | flops | bytes accessed | tf_op | source)
XLA Modules:
  0.0 155.1 jit_solution(16078153446316802775)
XLA Ops:
  0.0 152.8 %shard_map.118 = bf16[256,2048]{1,0:T(8,128)(2,1)} custom-call(bf16[256,2048]{1,0:T(8,128)(2,1)} %bitcast.4, f32[1,2048]{1,0:T(1,128)} %bitcast.5, bf16[256,128]{1,0:T(8,128)(2,1)} %w_key.1, bf16[256,128]{1,0:T(8,128)(2,1)} %w_value.1, bf16[256,1024]{1,0:T(8,128)(2,1)} %w_query.1, bf16[256,1024]{1,0:T(8,128)(2,1)} %w_cgate.1, bf16[256,1024]{1,0:T(8,128)(2,1)} %w_conv_in.1, ...), custom_call_target="tpu_custom_call" | custom-call | tf_op jit(solution)/shard_map/pallas_call | solution.py:755
  152.8 2.3 %copy.14 = bf16[1,256,2048]{2,1,0:T(8,128)(2,1)} copy(bf16[1,256,2048]{2,1,0:T(8,128)(2,1)} %bitcast.3) | data formatting | bytes 2097152

commit v3 on v2

--- a/solution.py
+++ b/solution.py
@@ -12,15 +12,16 @@
 TAPS = 3
 LANES = 128
 HALO = 16
-LEAD = 6
+LEAD = 3
+OUT_LEAD = 1
 MESH = pl.DeviceIdType.MESH
 
-KEYS = (2, 7, 10, 14)
-QUERY = (6, 8, 11, 15)
+KEYS = (2, 8, 11, 15)
+QUERY = (6, 9, 12, 16)
 ATTEND = (7, 11, 15, 19)
-GATE = (12, 13, 16, 17)
+GATE = (12, 13, 14, 17)
 GATED = (18, 19, 20, 21)
-RELAY = (4, 5, 8, 13)
+RELAY = (5, 6, 9, 14)
 
 epsilon = 1e-06
 
@@ -217,7 +218,12 @@
 
     above, below = jnp.minimum(s + 1, n - 1), jnp.maximum(s - 1, 0)
 
-    def own_start(k):
+    ready = set()
+
+    def own_ready(k):
+        if k in ready:
+            return
+        ready.add(k)
         if k < ins:
             j, h = k // m, k % m
             if h == 0:
@@ -235,6 +241,9 @@
                 @pl.when(f != h)
                 def _():
                     otrade_arrival(j, a, h).wait_recv()
+
+    def own_start(k):
+        own_ready(k)
 
         @pl.when(s < n - 1)
         def _():
@@ -349,6 +358,11 @@
         for k in range(1, Q):
             if (k // G) * (k % G) > 0:
                 tokens_on(nth(k))
+
+    def trade_out():
+        for j in range(2):
+            for a in range(A):
+                loop(1, m, lambda e: otrade(j, a, e).start())
 
     def tokens_sent():
         @pl.when(c == 0)
@@ -471,7 +485,13 @@
             return [(t // m, t % m, 0) for t in range(n * m)]
         if u == 0:
             return [(s, h, a) for h in range(m) for a in range(A)]
-        return [(other_plane(d), (u - 1) // A, (u - 1) % A) for d in range(1, n)]
+        k = min(u, m * A) - 1
+        planes = range(1, n)
+        if u == m * A:
+            planes = range(1, n - 1)
+        elif u > m * A:
+            planes = range(n - 1, n)
+        return [(other_plane(d), k // A, k % A) for d in planes]
 
     lists = [chunks_of(u) for u in range(U)]
     sizes = [len(chunks) * wa for chunks in lists]
@@ -539,7 +559,7 @@
         return here + precv[i, pl.ds(v * hr, hr), columns(u)].astype(jnp.float32)
 
     def stage_one(u):
-        loop(0, Q, lambda i: core_copy(u, i).wait_recv())
+        loop(1, Q, lambda k: core_copy(u, nth(k)).wait_recv())
         for v in range(2):
             n1, n2 = counts[v]
             for e in range(1, n1):
@@ -565,6 +585,7 @@
                 second_copy(u, v, i2).start()
 
     def stage_three(u):
+        core_copy(u, q).wait_recv()
         for v in range(2):
             value = with_first(u, v, 0)
             for i2 in range(1, counts[v][1]):
@@ -586,9 +607,6 @@
         own_start(k)
     normalize()
     tokens_first()
-    for j in range(2):
-        for a in range(A):
-            loop(1, m, lambda e: otrade(j, a, e).start())
     for k in range(LEAD):
         if k % m > 0:
             own_start(k)
@@ -639,6 +657,7 @@
         (place(RELAY[2]), functools.partial(tokens_relay, 0)),
         (place(RELAY[2]), functools.partial(tokens_direct, 1)),
         (place(RELAY[3]), tokens_far),
+        (place(RELAY[2] + 1), trade_out),
     ]
 
     def tasks(first, count, r):
@@ -654,35 +673,56 @@
                     index = jnp.where(r == t, k, index)
                 pl.when(hit)(functools.partial(run, nth(index) if whole else index))
 
-    stages = {"o": lambda u: loop(0, Q, lambda r: do_out(u, nth(r)))}
+    stages = {"o": lambda u: loop(1, Q + 1, lambda r: do_out(u, nth(lax.rem(r, Q))))}
     stages.update({"1": stage_one, "2": stage_two, "3": stage_three})
-    events = {}
+    def finish(k):
+        i = nth(lax.rem(k, Q))
+        do_conv(i)
+        do_out(0, i)
+
     last = U - 1
-    if U > 1:
-        for u in range(U):
-            if u > 0:
-                events.setdefault((ins + u - 1, n - 2), []).append(("o", u))
-            for name, k, r in (("1", ins + u, 1 if u == 0 else 0), ("2", ins + u + 1, 1), ("3", ins + u + 2, 1)):
-                if k < slots:
-                    events.setdefault((k, min(r, n - 2)), []).append((name, u))
+    after = {}
+    for u in range(U - 2):
+        k, low, high = ins + u, min(1, n - 2), n - 2
+        if u > 0:
+            after.setdefault((k, 0), []).append(("1", u))
+        after.setdefault((k + 1, low), []).append(("2", u))
+        after.setdefault((k + 2, low), []).append(("3", u))
+        if u < U - 3:
+            after.setdefault((k, high), []).append(("o", u + 1))
+    ending = (
+        [("2", last - 2), ("1", last), ("3", last - 3), ("2", last - 1)]
+        + [("3", last - 2), ("2", last), ("3", last - 1), ("3", last)]
+        if U > 1
+        else [("1", 0), ("2", 0), ("3", 0)]
+    )
 
     for k in range(slots):
-        if k + LEAD < slots:
-            own_start(k + LEAD)
+        for later in range(LEAD, slots):
+            if k == (later - LEAD if later < ins else max(later - OUT_LEAD, ins - LEAD)):
+                own_start(later)
         if k == ins and U == 1:
             loop(0, Q, lambda r: do_conv(nth(r)))
             tokens_sent()
         if k >= ins and U > 1:
             for r in range(n - 1):
                 if k == ins and r == 0:
-                    loop(0, Q // 2, lambda i: do_conv(nth(i)))
+                    for later in range(ins, slots):
+                        own_ready(later)
+                    tokens_sent()
+                    loop(1, Q // 2 + 1, finish)
                 if k == ins and r == 1:
-                    loop(Q // 2, Q, lambda i: do_conv(nth(i)))
-                    tokens_sent()
-                    stages["o"](0)
+                    loop(Q // 2 + 1, Q + 1, finish)
+                    stages["1"](0)
                 arrive(k, r + 1)
-                for name, u in sorted(events.get((k, r), []), key=lambda event: event[0]):
+                if k == slots - 1 and r == n - 3:
+                    stages["o"](last - 1)
+                for name, u in after.get((k, r), []):
                     stages[name](u)
+                if k == slots - 1 and r == n - 3:
+                    stages["1"](last - 1)
+                if k == slots - 1 and r == n - 2:
+                    stages["o"](last)
             continue
 
         def body(r):
@@ -693,9 +733,8 @@
         loop(0, n - 1, body)
     if U == 1:
         stages["o"](0)
-    for name, u in (("1", last), ("2", last - 1), ("3", last - 2), ("3", last - 1), ("2", last), ("3", last)):
-        if u >= 0:
-            stages[name](u)
+    for name, u in ending:
+        stages[name](u)
 
     for j in range(5):
         loop(1, m, lambda e: trade(j, e).wait_send())
@@ -744,7 +783,7 @@
     Q = m * G
     slim = width // Q
     A = 2 if across % (2 * LANES) == 0 else 1
-    U = m * A + 1 if across % LANES == 0 else 1
+    U = m * A + 2 if across % LANES == 0 else 1
     wa = across // A
     slots = 5 * m + m * A
     n1 = max(m, G) - 1

time: 155 us -> 148 us (0.955)
  Pallas kernels: 153 us -> 146 us
    pallas_call x1, Pallas kernels: 153 us -> 146 us  [local(): pl.pallas_call(functools.partial(kernel, G, n, m, A, U), out_shape=jax.Sh...]
where the time goes in v3:
time: 148 us
  Pallas kernels  146 us (99%)
  local copies, waits for them, and re-layouts  2.3 us (2%)
    pallas_call x1, Pallas kernels, local(): pl.pallas_call(functools.partial(kernel, G, n, m, A, U), out_shape=jax.Sh...  146 us

profile of v3, /device:TPU:0, one launch (start us, length us, event | category | flops | bytes accessed | tf_op | source)
XLA Modules:
  0.0 148.0 jit_solution(3235514317361594979)
XLA Ops:
  0.0 145.7 %shard_map.118 = bf16[256,2048]{1,0:T(8,128)(2,1)} custom-call(bf16[256,2048]{1,0:T(8,128)(2,1)} %bitcast.4, f32[1,2048]{1,0:T(1,128)} %bitcast.5, bf16[256,128]{1,0:T(8,128)(2,1)} %w_key.1, bf16[256,128]{1,0:T(8,128)(2,1)} %w_value.1, bf16[256,1024]{1,0:T(8,128)(2,1)} %w_query.1, bf16[256,1024]{1,0:T(8,128)(2,1)} %w_cgate.1, bf16[256,1024]{1,0:T(8,128)(2,1)} %w_conv_in.1, ...), custom_call_target="tpu_custom_call" | custom-call | tf_op jit(solution)/shard_map/pallas_call | solution.py:794
  145.7 2.3 %copy.14 = bf16[1,256,2048]{2,1,0:T(8,128)(2,1)} copy(bf16[1,256,2048]{2,1,0:T(8,128)(2,1)} %bitcast.3) | data formatting | bytes 2097152

commit v4 on v3

--- a/solution.py
+++ b/solution.py
@@ -794,7 +794,9 @@
     mixed = pl.pallas_call(
         functools.partial(kernel, G, n, m, A, U),
         out_shape=jax.ShapeDtypeStruct((own, features), bf16),
-        in_specs=[vmem] * 11 + [pl.BlockSpec(memory_space=pltpu.SMEM)],
+        in_specs=[vmem] * 4
+        + [pl.BlockSpec(memory_space=pl.ANY)] * 6
+        + [vmem, pl.BlockSpec(memory_space=pltpu.SMEM)],
         out_specs=vmem,
         scratch_shapes=[
             pltpu.VMEM((depth, 2 * kvwide), bf16),

time: 148 us -> 147 us (level)
  no operation moved by 1% of the time
where the time goes in v4:
time: 147 us
  Pallas kernels  145 us (99%)
  local copies, waits for them, and re-layouts  2.3 us (2%)
    pallas_call x1, Pallas kernels, local(): pl.pallas_call(functools.partial(kernel, G, n, m, A, U), out_shape=jax.Sh...  145 us

profile of v4, /device:TPU:0, one launch (start us, length us, event | category | flops | bytes accessed | tf_op | source)
XLA Modules:
  0.0 147.0 jit_solution(13152310273999832693)
XLA Ops:
  0.0 144.7 %shard_map.118 = bf16[256,2048]{1,0:T(8,128)(2,1)} custom-call(bf16[256,2048]{1,0:T(8,128)(2,1)} %bitcast.4, f32[1,2048]{1,0:T(1,128)} %bitcast.5, bf16[256,128]{1,0:T(8,128)(2,1)} %w_key.1, bf16[256,128]{1,0:T(8,128)(2,1)} %w_value.1, bf16[256,1024]{1,0:T(8,128)(2,1)} %w_query.1, bf16[256,1024]{1,0:T(8,128)(2,1)} %w_cgate.1, bf16[256,1024]{1,0:T(8,128)(2,1)} %w_conv_in.1, ...), custom_call_target="tpu_custom_call" | custom-call | tf_op jit(solution)/shard_map/pallas_call | solution.py:794
  144.7 2.3 %copy.14 = bf16[1,256,2048]{2,1,0:T(8,128)(2,1)} copy(bf16[1,256,2048]{2,1,0:T(8,128)(2,1)} %bitcast.3) | data formatting | bytes 2097152
